TPU v7x, 32 devices: a whole 2x2x4 slice. The times are simulated.
32 devices in a mesh: sp: 4 (over z), dp: 8 (over y, x, core).
Axes of the slice: x: 2, y: 2, z: 4, core: 2. Of those that a mesh axis runs over, the one named last changes fastest.
Arguments:
- value_half: bfloat16 [8, 1536, 2048], P('dp', 'sp'), may hold values from -6 to 6
- gate_half: bfloat16 [8, 1536, 2048], P('dp', 'sp'), may hold values from -9 to 9
- conv_taps: bfloat16 [31, 2048], replicated, may hold values from -1 to 1
- norm_gain: float32 [2048], replicated, may hold values from 0.1 to 1.9
- norm_shift: float32 [2048], replicated, may hold values from -3 to 3
- out_weight: bfloat16 [2048, 2048], P('dp', 'sp'), may hold values from -0.125 to 0.125
Outputs:
- module_out: bfloat16 [8, 1536, 2048], P('dp', 'sp')
All inputs are finite; a program needn't handle non-finite values.
Results may differ from a plain program's by a relative error of at most 0.0064.
Values may be sent and summed in bfloat16 or wider, within the bound.
A program may use at most 64 MiB of HBM per device.

v0:
```python
import jax
import jax.numpy as jnp
from jax import lax
from jax.sharding import PartitionSpec as P

EPSILON = 1e-06


def passed_along(value, axis, steps):
    count = lax.axis_size(axis)
    initial, last = (max(0, -steps), min(count, count - steps))
    return lax.ppermute(value, axis, [(source, source + steps) for source in range(initial, last)])


def causal_mix(padded, conv_taps, length):
    tap_count = conv_taps.shape[0]
    running = jnp.zeros((length, padded.shape[1]), jnp.float32)
    for tap_index in range(tap_count):
        running = running + padded[tap_index : tap_index + length].astype(jnp.float32) * conv_taps[
            tap_index
        ].astype(jnp.float32)
    return running.astype(jnp.bfloat16)


def per_device(value_half, gate_half, conv_taps, norm_gain, norm_shift, out_weight):
    tap_count = conv_taps.shape[0]
    tok_rows = value_half.shape[1]
    gated = (
        value_half[0].astype(jnp.float32) * jax.nn.sigmoid(gate_half[0].astype(jnp.float32))
    ).astype(jnp.bfloat16)
    tail_rows = gated[tok_rows - (tap_count - 1) :]
    history = passed_along(tail_rows, "sp", 1)
    padded = jnp.concatenate([history, gated], 0)
    convolved = causal_mix(padded, conv_taps, tok_rows)
    widened = convolved.astype(jnp.float32)
    mean_row = jnp.mean(widened, axis=-1, keepdims=True)
    centered = widened - mean_row
    variance = jnp.mean(centered * centered, axis=-1, keepdims=True)
    normed = centered * lax.rsqrt(variance + EPSILON) * norm_gain + norm_shift
    activated = jax.nn.silu(normed).astype(jnp.bfloat16)
    row_block = lax.all_gather(out_weight, "sp", axis=1, tiled=True)
    projected = jnp.dot(
        activated,
        lax.all_gather(row_block, "dp", axis=0, tiled=True),
        preferred_element_type=jnp.float32,
    )
    return projected.astype(jnp.bfloat16)[None]


def solution(mesh):
    placed = (P("dp", "sp", None), P("dp", "sp", None), P(), P(), P(), P("dp", "sp"))
    return jax.shard_map(
        per_device, mesh=mesh, in_specs=placed, out_specs=P("dp", "sp", None), check_vma=False
    )
```

profile of v0, /device:TPU:0, one launch (start us, length us, event | category | flops | bytes accessed | tf_op | source)
XLA Modules:
  0.0 110.5 jit_solution(4330929815768049006)
XLA Ops:
  6.5 0.0 copy-start
  6.5 0.0 all-gather.3.cloned.1.call-start
  6.5 0.7 all-gather.3.cloned.1.call-update
  7.3 0.0 all-gather.5.cloned.1.call-start
  7.3 32.3 %all-gather.3.cloned.1.call-done = bf16[256,2048]{1,0:T(8,128)(2,1)} async-done(((bf16[256,512]{1,0:T(8,128)(2,1)}), bf16[256,2048]{1,0:T(8,128)(2,1)}) %all-gather.3.cloned.1.call-update) | async-done | bytes 1048592 | tf_op jit(solution)/shard_map/all_gather | solution.py:41
  39.6 0.0 all-gather.5.cloned.1.call-update
  39.7 2.8 %multiply_convert_fusion = bf16[1,384,2048]{2,1,0:T(8,128)(2,1)S(1)} fusion(bf16[1,384,2048]{2,1,0:T(8,128)(2,1)} %param.6, bf16[1,384,2048]{2,1,0:T(8,128)(2,1)} %param.7), kind=kLoop, calls=%fused_computation.42 | loop fusion | flops 5505024 | bytes 4718592 | tf_op jit(solution)/shard_map/convert_element_type | solution.py:30
  42.5 0.0 copy-start.1
  42.5 0.0 copy-start.2
  42.5 3.4 %collective-permute-start = (bf16[30,2048]{1,0:T(8,128)(2,1)S(1)}, bf16[30,2048]{1,0:T(8,128)(2,1)S(1)}, u32[]{:S(2)}, u32[]{:S(2)}) collective-permute-start(bf16[30,2048]{1,0:T(8,128)(2,1)S(1)} %slice_bitcast_fusion), channel_id=1, source_target_pairs={{0,8},{8,16},{16,24},{1,9},{9,17},{17,25},{2,10},{10,18},{18,26},{... | collective-permute-start | bytes 368648 | tf_op jit(solution)/shard_map/ppermute | solution.py:12
  45.9 0.0 copy-done
  45.9 0.1 slice_convert_fusion.30
  46.0 0.1 slice_convert_fusion.29
  46.1 2.3 %collective-permute-done = bf16[30,2048]{1,0:T(8,128)(2,1)S(1)} collective-permute-done((bf16[30,2048]{1,0:T(8,128)(2,1)S(1)}, bf16[30,2048]{1,0:T(8,128)(2,1)S(1)}, u32[]{:S(2)}, u32[]{:S(2)}) %collective-permute-start) | collective-permute-done | bytes 122912 | tf_op jit(solution)/shard_map/ppermute | solution.py:12
  48.4 14.3 %convert_reduce_fusion = (f32[384]{0:T(512)S(1)}, bf16[384,2048]{1,0:T(8,128)(2,1)S(1)}) fusion(f32[2048]{0:T(1024)S(1)} %bitcast.67, bf16[384,2048]{1,0:T(8,128)(2,1)S(1)} %bitcast.37, f32[2048]{0:T(1024)S(1)} %bitcast.68, bf16[30,2048]{1,0:T(8,128)(2,1)S(1)} %collective-permute-done, f32[2048]{0:T(1024)S(1)} %bitcast.39, f32[2048]{0:T(1024)S(1)} %bitcast.40, ...), kind=kLoop, calls=%fused_computation.30 | loop fusion | flops 145489536 | bytes 3524096 | tf_op jit(solution)/shard_map/reduce_sum | solution.py:36
  62.7 0.6 fusion.2
  63.2 31.9 %all-gather.5.cloned.1.call-done = bf16[2048,2048]{1,0:T(8,128)(2,1)} async-done(((bf16[256,2048]{1,0:T(8,128)(2,1)}), bf16[2048,2048]{1,0:T(8,128)(2,1)}) %all-gather.5.cloned.1.call-update) | async-done | bytes 8388624 | tf_op jit(solution)/shard_map/all_gather | solution.py:44
  95.2 0.0 copy-done.1
  95.2 0.0 copy-done.2
  95.2 8.5 %fusion.11 = bf16[1,384,2048]{2,1,0:T(8,128)(2,1)} fusion(bf16[2048,2048]{1,0:T(8,128)(2,1)} %all-gather.5.cloned.1.call-done, bf16[384,2048]{1,0:T(8,128)(2,1)S(1)} %get-tuple-element.6, f32[2048]{0:T(1024)S(1)} %copy-done.1, f32[2048]{0:T(1024)S(1)} %copy-done.2, f32[384]{0:T(512)S(1)} %add_rsqrt_fusion, f32[384]{0:T(512)S(1)} %broadcast_multiply_fusion), kind=kOutput, calls=%fused_computation.45 | convolution fusion | flops 3229876224 | bytes 11553792 | tf_op jit(solution)/shard_map/dot_general | solution.py:42
  (3 shorter events, 0.0 us)
Async XLA Ops:
  6.5 39.4 %copy-start = (bf16[31,2048]{1,0:T(8,128)(2,1)S(1)}, bf16[31,2048]{1,0:T(8,128)(2,1)}, u32[]{:S(2)}) copy-start(bf16[31,2048]{1,0:T(8,128)(2,1)} %param.8) | copy-start | bytes 380932
  6.5 33.1 %all-gather.3.cloned.1.call-start = ((), (), s32[]{:S(2)}) async-start(), calls=%async_computation | async-start | bytes 1310720 | tf_op jit(solution)/shard_map/all_gather | solution.py:41
  7.3 87.9 %all-gather.5.cloned.1.call-start = ((), (), s32[]{:S(2)}) async-start(), calls=%async_computation.1 | async-start | bytes 9437184 | tf_op jit(solution)/shard_map/all_gather | solution.py:44
  42.5 52.7 %copy-start.1 = (f32[2048]{0:T(1024)S(1)}, f32[2048]{0:T(1024)}, u32[]{:S(2)}) copy-start(f32[2048]{0:T(1024)} %param.10) | copy-start | bytes 24580
  42.5 52.7 %copy-start.2 = (f32[2048]{0:T(1024)S(1)}, f32[2048]{0:T(1024)}, u32[]{:S(2)}) copy-start(f32[2048]{0:T(1024)} %param.9) | copy-start | bytes 24580
  42.5 5.9 %collective-permute-start = (bf16[30,2048]{1,0:T(8,128)(2,1)S(1)}, bf16[30,2048]{1,0:T(8,128)(2,1)S(1)}, u32[]{:S(2)}, u32[]{:S(2)}) collective-permute-start(bf16[30,2048]{1,0:T(8,128)(2,1)S(1)} %slice_bitcast_fusion), channel_id=1, source_target_pairs={{0,8},{8,16},{16,24},{1,9},{9,17},{17,25},{2,10},{10,18},{18,26},{... | collective-permute-start | bytes 368648 | tf_op jit(solution)/shard_map/ppermute | solution.py:12
Sparse Core Ops, SparseCore 0:
  8.9 30.6 all-gather.2
  41.5 53.6 all-gather.4
where the time goes:
time: 111 us
  waiting for transfers between devices  67.3 us (61%)
  other arithmetic  17.8 us (16%)
  between operations  13.5 us (12%)
  matrix products  8.49 us (8%)
  starting transfers between devices  3.4 us (3%)
    all_gather x1, waiting for transfers between devices, per_device(): row_block = lax.all_gather(out_weight, 'sp', axis=1, tiled=True)  32.3 us
    all_gather x1, waiting for transfers between devices, per_device(): lax.all_gather(row_block, 'dp', axis=0, tiled=True)  31.9 us
    reduce_sum x1, other arithmetic, per_device(): mean_row = jnp.mean(widened, axis=-1, keepdims=True)  14.3 us
    dot_general x1, matrix products, per_device(): jnp.dot(activated, lax.all_gather(row_block, 'dp', axis=0, tiled=True), p...  8.49 us
    ppermute x1, starting transfers between devices, passed_along(): lax.ppermute(value, axis, [(source, source + steps) for source in range(i...  3.36 us
    convert_element_type x1, other arithmetic, per_device(): gated = (value_half[0].astype(jnp.float32) * jax.nn.sigmoid(gate_half[0]....  2.79 us
    ppermute x1, waiting for transfers between devices, passed_along(): lax.ppermute(value, axis, [(source, source + steps) for source in range(i...  2.29 us
  transfers between devices with their start and end apart: 3, of which 3 were waited for; matrix products, arithmetic and copies ran while one was open for 16% of the time, Pallas kernels for 0%

commit v1 on v0

--- a/solution.py
+++ b/solution.py
@@ -38,7 +38,7 @@
     variance = jnp.mean(centered * centered, axis=-1, keepdims=True)
     normed = centered * lax.rsqrt(variance + EPSILON) * norm_gain + norm_shift
     activated = jax.nn.silu(normed).astype(jnp.bfloat16)
-    row_block = lax.all_gather(out_weight, "sp", axis=1, tiled=True)
+    row_block = jnp.concatenate(lax.all_gather(out_weight, "sp"), axis=1)
     projected = jnp.dot(
         activated,
         lax.all_gather(row_block, "dp", axis=0, tiled=True),

time: 111 us -> 114 us (1.027)
  local copies, waits for them, and re-layouts: 0.05 us -> 2.31 us
  other arithmetic: 17.8 us -> 15.9 us
  waiting for transfers between devices: 67.3 us -> 69.1 us
  matrix products: 8.49 us -> 10.1 us
    reshape x0 -> x1, local copies, waits for them, and re-layouts: none -> 2.26 us  [per_device(): row_block = jnp.concatenate(lax.all_gather(out_weight, 'sp'), axis=1)]
    convert_element_type x1, other arithmetic: 2.79 us -> 0.86 us  [per_device(): gated = (value_half[0].astype(jnp.float32) * jax.nn.sigmoid(gate_half[0]....]
    all_gather x1, waiting for transfers between devices: 31.9 us -> 33.7 us  [per_device(): lax.all_gather(row_block, 'dp', axis=0, tiled=True)]
    dot_general x1, matrix products: 8.49 us -> 10.1 us  [per_device(): jnp.dot(activated, lax.all_gather(row_block, 'dp', axis=0, tiled=True), p...]
  transfers between devices with their start and end apart: 3 -> 3, of which waited for: 3 -> 3; matrix products, arithmetic and copies ran while one was open for 16% -> 14% of each run, Pallas kernels for 0% -> 0%
where the time goes in v1:
time: 114 us
  waiting for transfers between devices  69.1 us (61%)
  other arithmetic  15.9 us (14%)
  between operations  13.5 us (12%)
  matrix products  10.1 us (9%)
  starting transfers between devices  3.4 us (3%)
  local copies, waits for them, and re-layouts  2.31 us (2%)
    all_gather x1, waiting for transfers between devices, per_device(): lax.all_gather(row_block, 'dp', axis=0, tiled=True)  33.7 us
    all_gather x1, waiting for transfers between devices, per_device(): row_block = jnp.concatenate(lax.all_gather(out_weight, 'sp'), axis=1)  32.3 us
    reduce_sum x1, other arithmetic, per_device(): mean_row = jnp.mean(widened, axis=-1, keepdims=True)  14.3 us
    dot_general x1, matrix products, per_device(): jnp.dot(activated, lax.all_gather(row_block, 'dp', axis=0, tiled=True), p...  10.1 us
    ppermute x1, starting transfers between devices, passed_along(): lax.ppermute(value, axis, [(source, source + steps) for source in range(i...  3.36 us
    ppermute x1, waiting for transfers between devices, passed_along(): lax.ppermute(value, axis, [(source, source + steps) for source in range(i...  2.29 us
  transfers between devices with their start and end apart: 3, of which 3 were waited for; matrix products, arithmetic and copies ran while one was open for 14% of the time, Pallas kernels for 0%

profile of v1, /device:TPU:0, one launch (start us, length us, event | category | flops | bytes accessed | tf_op | source)
XLA Modules:
  0.0 114.3 jit_solution(8431388869520999883)
XLA Ops:
  6.5 0.0 copy-start
  6.5 0.0 copy-start.1
  6.5 0.0 all-gather.6.cloned.1.call-start
  6.5 0.7 all-gather.6.cloned.1.call-update
  7.3 0.0 all-gather.4.cloned.1.call-start
  7.3 32.3 %all-gather.6.cloned.1.call-done = bf16[1024,512]{1,0:T(8,128)(2,1)} async-done(((bf16[256,512]{1,0:T(8,128)(2,1)}), bf16[1024,512]{1,0:T(8,128)(2,1)}) %all-gather.6.cloned.1.call-update) | async-done | bytes 1048592 | tf_op jit(solution)/shard_map/all_gather | solution.py:41
  39.6 2.3 %copy.7 = bf16[256,4,512]{0,2,1:T(8,128)(2,1)} copy(bf16[256,4,512]{2,0,1:T(8,128)(2,1)} %bitcast.43) | data formatting | bytes 2097152 | tf_op jit(solution)/shard_map/reshape | solution.py:41
  41.9 0.0 copy-start.2
  41.9 0.0 all-gather.4.cloned.1.call-update
  41.9 0.0 copy-done
  41.9 0.0 copy-done.1
  41.9 0.9 multiply_convert_fusion
  42.8 0.0 copy-start.3
  42.8 0.0 copy-start.4
  42.9 3.4 %collective-permute-start = (bf16[30,2048]{1,0:T(8,128)(2,1)S(1)}, bf16[30,2048]{1,0:T(8,128)(2,1)S(1)}, u32[]{:S(2)}, u32[]{:S(2)}) collective-permute-start(bf16[30,2048]{1,0:T(8,128)(2,1)S(1)} %slice_bitcast_fusion), channel_id=1, source_target_pairs={{0,8},{8,16},{16,24},{1,9},{9,17},{17,25},{2,10},{10,18},{18,26},{... | collective-permute-start | bytes 368648 | tf_op jit(solution)/shard_map/ppermute | solution.py:12
  46.3 0.0 copy-done.2
  46.3 0.1 slice_convert_fusion.30
  46.4 0.1 slice_convert_fusion.29
  46.5 2.3 %collective-permute-done = bf16[30,2048]{1,0:T(8,128)(2,1)S(1)} collective-permute-done((bf16[30,2048]{1,0:T(8,128)(2,1)S(1)}, bf16[30,2048]{1,0:T(8,128)(2,1)S(1)}, u32[]{:S(2)}, u32[]{:S(2)}) %collective-permute-start) | collective-permute-done | bytes 122912 | tf_op jit(solution)/shard_map/ppermute | solution.py:12
  48.7 14.3 %convert_reduce_fusion = (f32[384]{0:T(512)S(1)}, bf16[384,2048]{1,0:T(8,128)(2,1)S(1)}) fusion(f32[2048]{0:T(1024)S(1)} %bitcast.73, bf16[384,2048]{1,0:T(8,128)(2,1)S(1)} %bitcast.41, f32[2048]{0:T(1024)S(1)} %bitcast.74, bf16[30,2048]{1,0:T(8,128)(2,1)S(1)} %collective-permute-done, f32[2048]{0:T(1024)S(1)} %bitcast.45, f32[2048]{0:T(1024)S(1)} %bitcast.46, ...), kind=kLoop, calls=%fused_computation.30 | loop fusion | flops 145489536 | bytes 3524096 | tf_op jit(solution)/shard_map/reduce_sum | solution.py:36
  63.0 0.6 fusion.2
  63.6 33.7 %all-gather.4.cloned.1.call-done = bf16[2048,2048]{0,1:T(8,128)(2,1)} async-done(((bf16[256,2048]{0,1:T(8,128)(2,1)}), bf16[2048,2048]{0,1:T(8,128)(2,1)}) %all-gather.4.cloned.1.call-update) | async-done | bytes 8388624 | tf_op jit(solution)/shard_map/all_gather | solution.py:44
  97.3 0.0 copy-done.3
  97.3 0.0 copy-done.4
  97.3 10.1 %fusion.11 = bf16[1,384,2048]{2,1,0:T(8,128)(2,1)} fusion(bf16[2048,2048]{0,1:T(8,128)(2,1)} %all-gather.4.cloned.1.call-done, bf16[384,2048]{1,0:T(8,128)(2,1)S(1)} %get-tuple-element.6, f32[2048]{0:T(1024)S(1)} %copy-done.3, f32[2048]{0:T(1024)S(1)} %copy-done.4, f32[384]{0:T(512)S(1)} %add_rsqrt_fusion, f32[384]{0:T(512)S(1)} %broadcast_multiply_fusion), kind=kOutput, calls=%fused_computation.45 | convolution fusion | flops 3229876224 | bytes 11553792 | tf_op jit(solution)/shard_map/dot_general | solution.py:42
  (3 shorter events, 0.0 us)
Async XLA Ops:
  6.5 35.4 %copy-start = (bf16[1,384,2048]{2,1,0:T(8,128)(2,1)S(1)}, bf16[1,384,2048]{2,1,0:T(8,128)(2,1)}, u32[]{:S(2)}) copy-start(bf16[1,384,2048]{2,1,0:T(8,128)(2,1)} %param.6) | copy-start | bytes 4718596
  6.5 35.4 %copy-start.1 = (bf16[1,384,2048]{2,1,0:T(8,128)(2,1)S(1)}, bf16[1,384,2048]{2,1,0:T(8,128)(2,1)}, u32[]{:S(2)}) copy-start(bf16[1,384,2048]{2,1,0:T(8,128)(2,1)} %param.7) | copy-start | bytes 4718596
  6.5 33.1 %all-gather.6.cloned.1.call-start = ((), (), s32[]{:S(2)}) async-start(), calls=%async_computation.1 | async-start | bytes 1310720 | tf_op jit(solution)/shard_map/all_gather | solution.py:41
  7.3 90.1 %all-gather.4.cloned.1.call-start = ((), (), s32[]{:S(2)}) async-start(), calls=%async_computation | async-start | bytes 9437184 | tf_op jit(solution)/shard_map/all_gather | solution.py:44
  41.9 4.4 %copy-start.2 = (bf16[31,2048]{1,0:T(8,128)(2,1)S(1)}, bf16[31,2048]{1,0:T(8,128)(2,1)}, u32[]{:S(2)}) copy-start(bf16[31,2048]{1,0:T(8,128)(2,1)} %param.8) | copy-start | bytes 380932
  42.8 54.5 %copy-start.3 = (f32[2048]{0:T(1024)S(1)}, f32[2048]{0:T(1024)}, u32[]{:S(2)}) copy-start(f32[2048]{0:T(1024)} %param.10) | copy-start | bytes 24580
  42.8 54.5 %copy-start.4 = (f32[2048]{0:T(1024)S(1)}, f32[2048]{0:T(1024)}, u32[]{:S(2)}) copy-start(f32[2048]{0:T(1024)} %param.9) | copy-start | bytes 24580
  42.9 5.9 %collective-permute-start = (bf16[30,2048]{1,0:T(8,128)(2,1)S(1)}, bf16[30,2048]{1,0:T(8,128)(2,1)S(1)}, u32[]{:S(2)}, u32[]{:S(2)}) collective-permute-start(bf16[30,2048]{1,0:T(8,128)(2,1)S(1)} %slice_bitcast_fusion), channel_id=1, source_target_pairs={{0,8},{8,16},{16,24},{1,9},{9,17},{17,25},{2,10},{10,18},{18,26},{... | collective-permute-start | bytes 368648 | tf_op jit(solution)/shard_map/ppermute | solution.py:12
Sparse Core Ops, SparseCore 0:
  8.9 30.6 all-gather.5
  42.0 55.2 all-gather.3
